TPU v7x, 128 devices: a whole 4x4x4 slice. The times are simulated.
128 devices in a mesh: ep: 128 (over z, y, x, core).
Axes of the slice: x: 4, y: 4, z: 4, core: 2. Of those that a mesh axis runs over, the one named last changes fastest.
Arguments:
- hidden_in: bfloat16 [256, 2048], P('ep'), may hold values from -6 to 6
- lengths: int32 [256], P('ep'), may hold values from 1 to 1024, as said below
- key_cache: bfloat16 [256, 1024, 512], P('ep'), may hold values from -30 to 30
- value_cache: bfloat16 [256, 1024, 512], P('ep'), may hold values from -6 to 6
- query_w: bfloat16 [2048, 2048], P('ep'), may hold values from -0.125 to 0.125
- key_w: bfloat16 [2048, 512], P('ep'), may hold values from -0.125 to 0.125
- value_w: bfloat16 [2048, 512], P('ep'), may hold values from -0.125 to 0.125
- out_w: bfloat16 [2048, 2048], P('ep'), may hold values from -0.125 to 0.125
- lam_heads: float32 [8], replicated, may hold values from 0.3 to 0.8
- head_gain: float32 [256], replicated, may hold values from 0.1 to 1.9
- attn_gain: float32 [2048], replicated, may hold values from 0.1 to 1.9
- moe_gain: float32 [2048], replicated, may hold values from 0.1 to 1.9
- routing: int32 [256, 6], replicated, may hold values from 0 to 127, all different within a row; in each aligned block of 256 rows (0 to 255, 256 to 511, ...) at most 24 rows name the same one
- route_weight: float32 [256, 6], replicated, may hold values from 0.1 to 0.6
- gate_w: bfloat16 [128, 2048, 512], P('ep'), may hold values from -0.125 to 0.125
- up_w: bfloat16 [128, 2048, 512], P('ep'), may hold values from -0.125 to 0.125
- down_w: bfloat16 [128, 512, 2048], P('ep'), may hold values from -0.25 to 0.25
- shared_gate: bfloat16 [2048, 512], replicated, may hold values from -0.125 to 0.125
- shared_up: bfloat16 [2048, 512], replicated, may hold values from -0.125 to 0.125
- shared_down: bfloat16 [512, 2048], replicated, may hold values from -0.25 to 0.25
Outputs:
- layer_out: bfloat16 [256, 2048], P('ep')
- key_new: bfloat16 [256, 512], P('ep')
- value_new: bfloat16 [256, 512], P('ep')
Inputs may be any that keep to these rules, and one draw needn't show every extreme that they name: `lengths`: some sequence has exactly 1024 positions in use. `routing`: each row names 6 different experts; no expert is named by more than 24 rows, a bound that some block reaches.
All inputs are finite; a program needn't handle non-finite values.
Results may differ from a plain program's by a relative error of at most 0.013.
The roundings to bfloat16 on the way count: a program that leaves them out, or rounds other values in their place, can miss the bound.
Values may be sent and summed in bfloat16 or wider, within the bound.
A program may use at most 64 MiB of HBM per device.

v0:
```python
import jax
import jax.numpy as jnp
from jax import lax
from jax.sharding import Mesh
from jax.sharding import PartitionSpec as P

KV_HEADS = 2
HEAD_DIM = 128
EXP_CAP = 24
EP = ("ep_0", "ep_1", "ep_2", "ep_3")


eps_norm = 1e-06
eps_head = 1e-05
theta_base = 500000.0


def split_up(value, dim, length):
    dims = value.shape
    blocks = value.reshape(*dims[:dim], length, dims[dim] // length, *dims[dim + 1 :])
    return jnp.moveaxis(blocks, dim, 0)


def sent_and_summed(value, axis, dim):
    blocks = split_up(value, dim, lax.axis_size(axis))
    arrived = lax.all_to_all(blocks, axis, split_axis=0, concat_axis=0, tiled=True)
    return arrived.astype(jnp.float32).sum(axis=0)


def summed_rows(value, axes, dim):
    far, near = axes
    blocks = split_up(value, dim, lax.axis_size(far))
    nearer = sent_and_summed(blocks, near, dim + 1)
    arrived = lax.all_to_all(
        nearer.astype(jnp.bfloat16), far, split_axis=0, concat_axis=0, tiled=True
    )
    return arrived.astype(jnp.float32).sum(axis=0)


def rms_scale(row_block, gain_vec, epsilon):
    row_block = row_block.astype(jnp.float32)
    return (
        row_block
        * lax.rsqrt(jnp.mean(row_block * row_block, axis=-1, keepdims=True) + epsilon)
        * gain_vec
    )


def rotate(vectors, positions):
    half_width = vectors.shape[-1] // 2
    inverse = theta_base ** (-jnp.arange(half_width, dtype=jnp.float32) / half_width)
    angles = positions.astype(jnp.float32)[..., None] * inverse
    cosine, sine_part = (jnp.cos(angles), jnp.sin(angles))
    lower_half, upper_half = (vectors[..., :half_width], vectors[..., half_width:])
    return jnp.concatenate(
        [
            lower_half * cosine - upper_half * sine_part,
            lower_half * sine_part + upper_half * cosine,
        ],
        axis=-1,
    )


def attend(queries, key_new, value_new, cache_keys, cache_values, lengths, lam_heads, head_gain):
    num_seqs, kv_heads, group_size = (queries.shape[0], queries.shape[1], queries.shape[2])
    head_dim = queries.shape[-1]
    cache_len = cache_keys.shape[1]
    cache_keys = cache_keys.reshape(num_seqs, cache_len, kv_heads, 2, head_dim)
    cache_values = cache_values.reshape(num_seqs, cache_len, kv_heads, -1)
    value_new = value_new.reshape(num_seqs, kv_heads, -1)
    score_scale = head_dim ** (-0.5)
    scores = (
        jnp.einsum("skgph,sckph->skgpc", queries, cache_keys, preferred_element_type=jnp.float32)
        * score_scale
    )
    self_score = (
        jnp.einsum("skgph,skph->skgp", queries, key_new, preferred_element_type=jnp.float32)
        * score_scale
    )
    live_mask = (jnp.arange(cache_len)[None, :] < lengths[:, None])[:, None, None, None, :]
    peak = jnp.maximum(jnp.max(jnp.where(live_mask, scores, -jnp.inf), axis=-1), self_score)
    weights = jnp.where(live_mask, jnp.exp(scores - peak[..., None]), 0.0)
    self_weight = jnp.exp(self_score - peak)
    totals = jnp.sum(weights, axis=-1) + self_weight
    lambda_grid = lam_heads.reshape(kv_heads, group_size)[None]
    combined = (
        weights[:, :, :, 0] / totals[:, :, :, 0, None]
        - lambda_grid[..., None] * weights[:, :, :, 1] / totals[:, :, :, 1, None]
    ).astype(jnp.bfloat16)
    self_combined = (
        self_weight[..., 0] / totals[..., 0] - lambda_grid * self_weight[..., 1] / totals[..., 1]
    ).astype(jnp.bfloat16)
    head_out = jnp.einsum(
        "skgc,sckv->skgv", combined, cache_values, preferred_element_type=jnp.float32
    )
    head_out = (
        head_out
        + self_combined.astype(jnp.float32)[..., None]
        * value_new.astype(jnp.float32)[:, :, None, :]
    )
    return rms_scale(head_out, head_gain, eps_head).astype(jnp.bfloat16).reshape(num_seqs, -1)


def expert_rows(row_block, routed_here, gate_one, up_one, down_one):
    slot_index = jnp.cumsum(routed_here) - 1
    pick_table = (
        (slot_index[None, :] == jnp.arange(EXP_CAP)[:, None]) & (routed_here[None, :] > 0)
    ).astype(jnp.bfloat16)
    picked = jnp.dot(pick_table, row_block, preferred_element_type=jnp.float32).astype(jnp.bfloat16)
    hidden = (
        jax.nn.silu(jnp.dot(picked, gate_one, preferred_element_type=jnp.float32))
        * jnp.dot(picked, up_one, preferred_element_type=jnp.float32)
    ).astype(jnp.bfloat16)
    result = jnp.dot(hidden, down_one, preferred_element_type=jnp.float32).astype(jnp.bfloat16)
    return jnp.dot(pick_table.T, result, preferred_element_type=jnp.float32)


def on_device(
    hidden_in,
    lengths,
    key_cache,
    value_cache,
    query_w,
    key_w,
    value_w,
    out_w,
    lam_heads,
    head_gain,
    attn_gain,
    moe_gain,
    routing,
    route_weight,
    gate_w,
    up_w,
    down_w,
    shared_gate,
    shared_up,
    shared_down,
):
    devices = lax.axis_size(EP)
    device = lax.axis_index(EP)
    tok_dev = hidden_in.shape[0]
    model_width = hidden_in.shape[1]
    all_rows = lax.all_gather(hidden_in, EP, axis=0, tiled=True)
    normed = rms_scale(all_rows, attn_gain, eps_norm).astype(jnp.bfloat16)
    joined_rows = jnp.concatenate([query_w, key_w, value_w], axis=1)
    column_block = lax.all_to_all(joined_rows, EP, split_axis=1, concat_axis=0, tiled=True)
    column_sums = jnp.dot(normed, column_block, preferred_element_type=jnp.float32)
    projected = lax.all_to_all(column_sums, EP, split_axis=0, concat_axis=1, tiled=True)
    query_cols = query_w.shape[1]
    key_cols = key_w.shape[1]
    queries = rotate(
        projected[:, :query_cols].reshape(tok_dev, KV_HEADS, -1, 2, HEAD_DIM),
        lengths[:, None, None, None],
    ).astype(jnp.bfloat16)
    key_new = rotate(
        projected[:, query_cols : query_cols + key_cols].reshape(tok_dev, KV_HEADS, 2, HEAD_DIM),
        lengths[:, None, None],
    ).astype(jnp.bfloat16)
    value_new = projected[:, query_cols + key_cols :].astype(jnp.bfloat16)
    attn_out = attend(
        queries, key_new, value_new, key_cache, value_cache, lengths, lam_heads, head_gain
    )
    pieces = lax.all_to_all(attn_out, EP, split_axis=1, concat_axis=0, tiled=True)
    routed_here = jnp.sum((routing == device).astype(jnp.int32), axis=1)
    attn_proj = summed_rows(
        jnp.dot(pieces, out_w, preferred_element_type=jnp.float32).astype(jnp.bfloat16),
        (("ep_0", "ep_1", "ep_2"), "ep_3"),
        0,
    ).astype(jnp.bfloat16)
    after_mixer = (hidden_in.astype(jnp.float32) + attn_proj.astype(jnp.float32)).astype(
        jnp.bfloat16
    )
    moe_in = rms_scale(after_mixer, moe_gain, eps_norm).astype(jnp.bfloat16)
    own_routes = lax.dynamic_slice_in_dim(routing, device * tok_dev, tok_dev, 0)
    own_weights = lax.dynamic_slice_in_dim(route_weight, device * tok_dev, tok_dev, 0)
    expert_ids = jnp.arange(devices, dtype=jnp.int32)
    matches = own_routes[:, :, None] == expert_ids[None, None, :]
    chosen = jnp.any(matches, axis=1)
    weight_grid = jnp.sum(jnp.where(matches, own_weights[:, :, None], 0.0), axis=1)
    outgoing = jnp.where(chosen.T[:, :, None], moe_in[None], jnp.zeros((), jnp.bfloat16))
    arrived = lax.all_to_all(outgoing, EP, split_axis=0, concat_axis=0, tiled=True)
    result = expert_rows(
        arrived.reshape(devices * tok_dev, model_width), routed_here, gate_w[0], up_w[0], down_w[0]
    ).astype(jnp.bfloat16)
    returned = lax.all_to_all(
        result.reshape(devices, tok_dev, model_width), EP, split_axis=0, concat_axis=0, tiled=True
    )
    routed = jnp.sum(returned.astype(jnp.float32) * weight_grid.T[:, :, None], axis=0)
    shared_hidden = (
        jax.nn.silu(jnp.dot(moe_in, shared_gate, preferred_element_type=jnp.float32))
        * jnp.dot(moe_in, shared_up, preferred_element_type=jnp.float32)
    ).astype(jnp.bfloat16)
    shared_out = jnp.dot(shared_hidden, shared_down, preferred_element_type=jnp.float32)
    layer_out = (after_mixer.astype(jnp.float32) + routed + shared_out).astype(jnp.bfloat16)
    return (layer_out, key_new.reshape(tok_dev, -1), value_new)


def solution(mesh):
    torus = Mesh(mesh.devices.reshape(4, 4, 4, 2), ("ep_0", "ep_1", "ep_2", "ep_3"))
    return jax.shard_map(
        on_device,
        mesh=torus,
        in_specs=(
            P(EP, None),
            P(EP),
            P(EP, None, None),
            P(EP, None, None),
            P(EP, None),
            P(EP, None),
            P(EP, None),
            P(EP, None),
            P(),
            P(),
            P(),
            P(),
            P(),
            P(),
            P(EP, None, None),
            P(EP, None, None),
            P(EP, None, None),
            P(),
            P(),
            P(),
        ),
        out_specs=(P(EP, None), P(EP, None), P(EP, None)),
        check_vma=False,
    )
```

profile of v0, /device:TPU:1, one launch (start us, length us, event | category | flops | bytes accessed | tf_op | source)
XLA Modules:
  0.0 221.3 jit_solution(17257553948698546519)
XLA Ops:
  10.0 1.2 reshape.270
  11.2 11.5 %all-to-all-start = ((bf16[128,2,192]{2,1,0:T(2,128)(2,1)}), bf16[128,2,192]{2,1,0:T(2,128)(2,1)S(1)}, u32[]{:S(2)}, u32[]{:S(2)}) async-start(bf16[128,2,192]{2,1,0:T(2,128)(2,1)} %reshape.270), calls=%async_computation | async-start | bytes 262144 | tf_op jit(solution)/shard_map/all_to_all | solution.py:147
  22.8 9.9 %all-to-all-done = bf16[128,2,192]{2,1,0:T(2,128)(2,1)S(1)} async-done(((bf16[128,2,192]{2,1,0:T(2,128)(2,1)}), bf16[128,2,192]{2,1,0:T(2,128)(2,1)S(1)}, u32[]{:S(2)}, u32[]{:S(2)}) %all-to-all-start) | async-done | bytes 98336 | tf_op jit(solution)/shard_map/all_to_all | solution.py:147
  32.7 1.2 reshape.271
  33.9 44.1 %all-gather.3.cloned.1.call-done = bf16[128,2,2048]{2,1,0:T(2,128)(2,1)} async-done(((bf16[1,2,2048]{2,1,0:T(2,128)(2,1)}), bf16[128,2,2048]{2,1,0:T(2,128)(2,1)}) %all-gather.3.cloned.1.call-update) | async-done | bytes 1048592 | tf_op jit(solution)/shard_map/all_gather | solution.py:144
  78.0 2.5 %reshape.265 = f32[256,2048]{1,0:T(8,128)} reshape(bf16[128,2,2048]{2,1,0:T(2,128)(2,1)} %all-gather.3.cloned.1.call-done) | data formatting | bytes 3145728 | tf_op jit(solution)/shard_map/convert_element_type | solution.py:41
  80.6 2.0 multiply_reduce_fusion.1
  83.0 1.5 dot_general.41
  84.5 2.1 fusion.29
  87.4 5.4 %all-to-all-start.1 = ((f32[128,2,24]{2,1,0:T(2,128)}), f32[128,2,24]{2,1,0:T(2,128)S(1)}, u32[]{:S(2)}, u32[]{:S(2)}) async-start(f32[128,2,24]{2,1,0:T(2,128)} %copy.77), calls=%async_computation.1 | async-start | bytes 262144 | tf_op jit(solution)/shard_map/all_to_all | solution.py:149
  92.9 4.0 %reshape.254 = bf16[2,1024,2,2,128]{4,3,2,1,0:T(2,128)(2,1)} reshape(bf16[2,1024,512]{2,1,0:T(8,128)(2,1)} %param.22) | data formatting | bytes 4194304 | tf_op jit(solution)/shard_map/reshape | solution.py:68
  96.9 5.8 %all-to-all-done.1 = f32[128,2,24]{2,1,0:T(2,128)S(1)} async-done(((f32[128,2,24]{2,1,0:T(2,128)}), f32[128,2,24]{2,1,0:T(2,128)S(1)}, u32[]{:S(2)}, u32[]{:S(2)}) %all-to-all-start.1) | async-done | bytes 24608 | tf_op jit(solution)/shard_map/all_to_all | solution.py:149
  103.5 2.4 %select_reduce_fusion = (f32[2,2,4,2]{2,3,1,0:T(2,128)S(1)}, f32[2,2,4,2,1024]{4,2,3,1,0:T(4,128)S(1)}) fusion(pred[2,1024]{1,0:T(4,128)(4,1)S(1)} %iota_compare_fusion.1, bf16[2,1024,2,2,128]{4,3,2,1,0:T(2,128)(2,1)} %reshape.254, bf16[2,2,4,2,64]{4,2,3,1,0:T(4,128)(2,1)S(1)} %get-tuple-element.8, bf16[2,2,4,2,64]{4,2,3,1,0:T(4,128)(2,1)S(1)} %get-tuple-element.7), kind=kOutput, calls=%fused_computation.31 | convolution fusion | flops 8503264 | bytes 2238592 | tf_op jit(solution)/shard_map/skgph,sckph->skgpc/dot_general | solution.py:73
  106.1 2.1 multiply_reduce_fusion.2
  108.5 13.7 %all_to_all.74 = bf16[2,128,16]{2,0,1:T(2,128)(2,1)S(1)} all-to-all(bf16[2,128,16]{2,0,1:T(2,128)(2,1)S(1)} %copy.84), channel_id=1, replica_groups=mesh['ep_0'=4,'ep_1'=4,'ep_2'=4,'ep_3'=2] {'ep_0','ep_1','ep_2','ep_3'}, dimensions={1} | all-to-all | bytes 16384 | tf_op jit(solution)/shard_map/all_to_all | solution.py:164
  122.6 1.5 reshape_reshape.3
  124.1 1.9 copy.125
  126.0 5.0 %all_to_all.75 = bf16[2,64,2,2048]{3,2,1,0:T(2,128)(2,1)S(1)} all-to-all(bf16[2,64,2,2048]{3,2,1,0:T(2,128)(2,1)S(1)} %bitcast.97), channel_id=1, replica_groups=mesh['ep_0'=4,'ep_1'=4,'ep_2'=4,'ep_3'=2] {'ep_3'}, dimensions={0} | all-to-all | bytes 2097152 | tf_op jit(solution)/shard_map/all_to_all | solution.py:26
  131.0 3.1 %reduce_sum.90 = bf16[64,2,2048]{2,1,0:T(2,128)(2,1)} reduce(bf16[2,64,2,2048]{3,2,1,0:T(2,128)(2,1)S(1)} %all_to_all.75, bf16[]{:T(256)} %constant.30.clone.1), dimensions={0}, to_apply=%region_4.5 | reduce | flops 262144 | bytes 1572866 | tf_op jit(solution)/shard_map/reduce_sum | solution.py:27
  134.1 4.9 %all-to-all-start.4 = ((bf16[64,2,2048]{2,1,0:T(2,128)(2,1)}), bf16[64,2,2048]{2,1,0:T(2,128)(2,1)S(1)}, u32[]{:S(2)}, u32[]{:S(2)}) async-start(bf16[64,2,2048]{2,1,0:T(2,128)(2,1)} %reduce_sum.90), calls=%async_computation.4 | async-start | bytes 1048576 | tf_op jit(solution)/shard_map/all_to_all | solution.py:34
  139.3 12.1 %all-to-all-done.4 = bf16[64,2,2048]{2,1,0:T(2,128)(2,1)S(1)} async-done(((bf16[64,2,2048]{2,1,0:T(2,128)(2,1)}), bf16[64,2,2048]{2,1,0:T(2,128)(2,1)S(1)}, u32[]{:S(2)}, u32[]{:S(2)}) %all-to-all-start.4) | async-done | bytes 524320 | tf_op jit(solution)/shard_map/all_to_all | solution.py:34
  152.1 1.8 broadcast_select_fusion
  153.9 5.3 %all-to-all-start.5 = ((bf16[128,2,2048]{2,1,0:T(2,128)(2,1)}), bf16[128,2,2048]{2,1,0:T(2,128)(2,1)S(1)}, u32[]{:S(2)}, u32[]{:S(2)}) async-start(bf16[128,2,2048]{2,1,0:T(2,128)(2,1)} %broadcast_select_fusion), calls=%async_computation.5 | async-start | bytes 2097152 | tf_op jit(solution)/shard_map/all_to_all | solution.py:182
  159.8 18.7 %all-to-all-done.5 = bf16[128,2,2048]{2,1,0:T(2,128)(2,1)S(1)} async-done(((bf16[128,2,2048]{2,1,0:T(2,128)(2,1)}), bf16[128,2,2048]{2,1,0:T(2,128)(2,1)S(1)}, u32[]{:S(2)}, u32[]{:S(2)}) %all-to-all-start.5) | async-done | bytes 1048608 | tf_op jit(solution)/shard_map/all_to_all | solution.py:182
  178.6 1.2 reshape.259
  179.8 1.6 convolution_convert_fusion.3
  181.4 2.0 fusion.7
  184.5 1.5 reshape.260
  186.0 4.4 %all-to-all-start.6 = ((bf16[128,2,2048]{2,1,0:T(2,128)(2,1)}), bf16[128,2,2048]{2,1,0:T(2,128)(2,1)S(1)}, u32[]{:S(2)}, u32[]{:S(2)}) async-start(bf16[128,2,2048]{2,1,0:T(2,128)(2,1)} %reshape.260), calls=%async_computation.6 | async-start | bytes 2097152 | tf_op jit(solution)/shard_map/all_to_all | solution.py:186
  191.4 2.0 fusion.62
  193.4 16.4 %all-to-all-done.6 = bf16[128,2,2048]{2,1,0:T(2,128)(2,1)S(1)} async-done(((bf16[128,2,2048]{2,1,0:T(2,128)(2,1)}), bf16[128,2,2048]{2,1,0:T(2,128)(2,1)S(1)}, u32[]{:S(2)}, u32[]{:S(2)}) %all-to-all-start.6) | async-done | bytes 1048608 | tf_op jit(solution)/shard_map/all_to_all | solution.py:186
  210.9 3.6 %fusion = bf16[2,2048]{1,0:T(2,128)(2,1)} fusion(bf16[512,2048]{1,0:T(8,128)(2,1)} %param.39, bf16[2,2048]{1,0:T(2,128)(2,1)S(1)} %fusion.42, bf16[2048,512]{1,0:T(8,128)(2,1)} %param.38, f32[2,2048]{1,0:T(2,128)S(1)} %multiply_reduce_fusion, f32[2,512]{1,0:T(2,128)S(1)} %fusion.62, bf16[2,2048]{1,0:T(2,128)(2,1)S(1)} %reduce_sum.91, ...), kind=kOutput, calls=%fused_computation.5 | convolution fusion | flops 8427520 | bytes 4247552 | tf_op jit(solution)/shard_map/dot_general | solution.py:194
  (83 shorter events, 10.7 us)
Async XLA Ops:
  7.2 176.6 %copy-start = (bf16[1,512,2048]{2,1,0:T(8,128)(2,1)S(1)}, bf16[1,512,2048]{2,1,0:T(8,128)(2,1)}, u32[]{:S(2)}) copy-start(bf16[1,512,2048]{2,1,0:T(8,128)(2,1)} %param.36) | copy-start | bytes 6291460
  7.2 15.5 %copy-start.11 = (s32[2]{0:T(128)S(1)}, s32[2]{0:T(128)}, u32[]{:S(2)}) copy-start(s32[2]{0:T(128)} %param.21) | copy-start | bytes 28
  7.2 70.8 %all-gather.3.cloned.1.call-start = ((), (), s32[]{:S(2)}) async-start(), calls=%async_computation.7 | async-start | bytes 1056768 | tf_op jit(solution)/shard_map/all_gather | solution.py:144
  11.2 21.5 %all-to-all-start = ((bf16[128,2,192]{2,1,0:T(2,128)(2,1)}), bf16[128,2,192]{2,1,0:T(2,128)(2,1)S(1)}, u32[]{:S(2)}, u32[]{:S(2)}) async-start(bf16[128,2,192]{2,1,0:T(2,128)(2,1)} %reshape.270), calls=%async_computation | async-start | bytes 262144 | tf_op jit(solution)/shard_map/all_to_all | solution.py:147
  33.9 48.7 %copy-start.6 = (f32[2048]{0:T(1024)S(1)}, f32[2048]{0:T(1024)}, u32[]{:S(2)}) copy-start(f32[2048]{0:T(1024)} %param.30) | copy-start | bytes 24580
  80.6 2.2 %copy-start.1 = (f32[256,2048]{1,0:T(8,128)S(1)}, f32[256,2048]{1,0:T(8,128)}, u32[]{:S(2)}) copy-start(f32[256,2048]{1,0:T(8,128)} %reshape.265) | copy-start | bytes 6291460
  87.4 15.4 %all-to-all-start.1 = ((f32[128,2,24]{2,1,0:T(2,128)}), f32[128,2,24]{2,1,0:T(2,128)S(1)}, u32[]{:S(2)}, u32[]{:S(2)}) async-start(f32[128,2,24]{2,1,0:T(2,128)} %copy.77), calls=%async_computation.1 | async-start | bytes 262144 | tf_op jit(solution)/shard_map/all_to_all | solution.py:149
  92.9 4.0 %copy-start.12 = (f32[8]{0:T(128)S(1)}, f32[8]{0:T(128)}, u32[]{:S(2)}) copy-start(f32[8]{0:T(128)} %param.28) | copy-start | bytes 100
  102.9 5.3 %copy-start.7 = (bf16[2,512]{1,0:T(2,128)(2,1)}, bf16[2,512]{1,0:T(2,128)(2,1)S(1)}, u32[]{:S(2)}) copy-start(bf16[2,512]{1,0:T(2,128)(2,1)S(1)} %slice.111) | copy-start | bytes 6148
  105.8 2.4 %copy-start.10 = (f32[256]{0:T(256)S(1)}, f32[256]{0:T(256)}, u32[]{:S(2)}) copy-start(f32[256]{0:T(256)} %param.29) | copy-start | bytes 3076
  105.8 16.3 %copy-start.4 = (bf16[16,2048]{1,0:T(8,128)(2,1)S(1)}, bf16[16,2048]{1,0:T(8,128)(2,1)}, u32[]{:S(2)}) copy-start(bf16[16,2048]{1,0:T(8,128)(2,1)} %param.27) | copy-start | bytes 196612
  126.0 13.0 %copy-start.5 = (s32[256,6]{0,1:T(8,128)S(1)}, s32[256,6]{0,1:T(8,128)}, u32[]{:S(2)}) copy-start(s32[256,6]{0,1:T(8,128)} %param.32) | copy-start | bytes 18436
  131.0 20.9 %copy-start.3 = (bf16[2,2048]{1,0:T(2,128)(2,1)S(1)}, bf16[2,2048]{1,0:T(2,128)(2,1)}, u32[]{:S(2)}) copy-start(bf16[2,2048]{1,0:T(2,128)(2,1)} %param.20) | copy-start | bytes 24580
  131.0 21.0 %copy-start.8 = (f32[2048]{0:T(1024)S(1)}, f32[2048]{0:T(1024)}, u32[]{:S(2)}) copy-start(f32[2048]{0:T(1024)} %param.31) | copy-start | bytes 24580
  134.1 17.3 %all-to-all-start.4 = ((bf16[64,2,2048]{2,1,0:T(2,128)(2,1)}), bf16[64,2,2048]{2,1,0:T(2,128)(2,1)S(1)}, u32[]{:S(2)}, u32[]{:S(2)}) async-start(bf16[64,2,2048]{2,1,0:T(2,128)(2,1)} %reduce_sum.90), calls=%async_computation.4 | async-start | bytes 1048576 | tf_op jit(solution)/shard_map/all_to_all | solution.py:34
  153.9 24.7 %all-to-all-start.5 = ((bf16[128,2,2048]{2,1,0:T(2,128)(2,1)}), bf16[128,2,2048]{2,1,0:T(2,128)(2,1)S(1)}, u32[]{:S(2)}, u32[]{:S(2)}) async-start(bf16[128,2,2048]{2,1,0:T(2,128)(2,1)} %broadcast_select_fusion), calls=%async_computation.5 | async-start | bytes 2097152 | tf_op jit(solution)/shard_map/all_to_all | solution.py:182
  179.8 3.6 %copy-start.2 = (bf16[1,2048,512]{2,1,0:T(8,128)(2,1)S(1)}, bf16[1,2048,512]{2,1,0:T(8,128)(2,1)}, u32[]{:S(2)}) copy-start(bf16[1,2048,512]{2,1,0:T(8,128)(2,1)} %param.35) | copy-start | bytes 6291460
  184.5 6.0 %copy-start.9 = (f32[256,6]{0,1:T(8,128)S(1)}, f32[256,6]{0,1:T(8,128)}, u32[]{:S(2)}) copy-start(f32[256,6]{0,1:T(8,128)} %param.33) | copy-start | bytes 18436
  186.0 23.8 %all-to-all-start.6 = ((bf16[128,2,2048]{2,1,0:T(2,128)(2,1)}), bf16[128,2,2048]{2,1,0:T(2,128)(2,1)S(1)}, u32[]{:S(2)}, u32[]{:S(2)}) async-start(bf16[128,2,2048]{2,1,0:T(2,128)(2,1)} %reshape.260), calls=%async_computation.6 | async-start | bytes 2097152 | tf_op jit(solution)/shard_map/all_to_all | solution.py:186
Sparse Core Ops, SparseCore 0:
  10.8 67.1 all-gather.2
where the time goes:
time: 222 us; the launch traced here: 221 us
  waiting for transfers between devices  108 us (49%)
  starting transfers between devices  31.5 us (14%)
  local copies, waits for them, and re-layouts  20.6 us (9%)
  blocking collectives  18.6 us (8%)
  matrix products  17.3 us (8%)
  between operations  14.3 us (6%)
  other arithmetic  11.2 us (5%)
    all_gather x1, waiting for transfers between devices, on_device(): all_rows = lax.all_gather(hidden_in, EP, axis=0, tiled=True)  44.1 us
    all_to_all x1, waiting for transfers between devices, on_device(): lax.all_to_all(outgoing, EP, split_axis=0, concat_axis=0, tiled=True)  18.7 us
    all_to_all x1, waiting for transfers between devices, on_device(): lax.all_to_all(result.reshape(devices, tok_dev, model_width), EP, split_a...  16.4 us
    all_to_all x1, blocking collectives, on_device(): lax.all_to_all(attn_out, EP, split_axis=1, concat_axis=0, tiled=True)  13.7 us
    all_to_all x1, waiting for transfers between devices, summed_rows(): lax.all_to_all(nearer.astype(jnp.bfloat16), far, split_axis=0, concat_axi...  12.1 us
    all_to_all x1, starting transfers between devices, on_device(): lax.all_to_all(joined_rows, EP, split_axis=1, concat_axis=0, tiled=True)  11.5 us
    all_to_all x1, waiting for transfers between devices, on_device(): lax.all_to_all(joined_rows, EP, split_axis=1, concat_axis=0, tiled=True)  9.9 us
    all_to_all x1, waiting for transfers between devices, on_device(): lax.all_to_all(column_sums, EP, split_axis=0, concat_axis=1, tiled=True)  5.83 us
  transfers between devices with their start and end apart: 6, of which 6 were waited for; matrix products, arithmetic and copies ran while one was open for 5% of the time, Pallas kernels for 0%

commit v1 on v0

v1 whole, which is shorter than its diff:
```python
import functools

import jax
import jax.numpy as jnp
import numpy as np
from jax import lax
from jax.experimental import pallas as pl
from jax.experimental.pallas import tpu as pltpu
from jax.sharding import PartitionSpec as P

MESH = pl.DeviceIdType.MESH
F32 = jnp.float32
BF16 = jnp.bfloat16
SIDE = 4
CHIPS = SIDE**3
PLANE = SIDE * SIDE * 2
SLOTS = 32
D = 2048
eps_norm = 1e-06
eps_head = 1e-05
theta_base = 500000.0


def bytes_of(buf, count, sem):
    part = buf.at[pl.ds(0, count)]
    pltpu.make_async_copy(part, part, sem).wait()


def row_parity():
    return lax.broadcasted_iota(jnp.int32, (32, 128), 0) % 2


def fold_rms(fold, gain):
    parity = row_parity()
    squares = fold * fold
    first = jnp.sum(jnp.where(parity == 0, squares, 0.0), keepdims=True)
    second = jnp.sum(jnp.where(parity == 1, squares, 0.0), keepdims=True)
    r0 = lax.rsqrt(first * (1.0 / D) + eps_norm)
    r1 = lax.rsqrt(second * (1.0 / D) + eps_norm)
    return fold * jnp.where(parity == 0, r0, r1) * gain


def kernel(
    len_ref, lam_ref, hidden_ref, inv_ref, again_ref, mgain_ref, hgain_ref, routing_ref, rweight_ref,
    kc_hbm, vc_hbm, qw_hbm, kw_hbm, vw_hbm, ow_hbm, gate_hbm, up_hbm, down_hbm, sg_hbm, su_hbm, sd_hbm,
    layer_ref, kout_ref, vout_ref,
    kc, vc, gate, up, down, sg, su, sd,
    wcat, owcat, wrecv, owrecv,
    hid, gdup, asend, acts, xf, p2, qkv_in, qs,
    af, asend2, acts2, p5, oin, proj,
    ms, mrecv, big, pk, rs, rpar, esend, erecv, es, shf, rfold,
    pt, ptt, wtok, ptmp,
    local_sem, send_sem, recv_sem,
):
    me = lax.axis_index("ep")
    c = me % 2
    p = me // 2
    x = p % SIDE
    y = (p // SIDE) % SIDE
    z = p // (SIDE * SIDE)
    xc = x * 2 + c
    partner = me + 1 - 2 * c
    o_me = z * 8 + xc
    w_me = y * 8 + xc

    def local(src, dst, k):
        cp = pltpu.make_async_copy(src, dst, local_sem.at[k])
        cp.start()
        return cp

    def remote(src, dst, k, target):
        pltpu.make_async_remote_copy(
            src_ref=src,
            dst_ref=dst,
            send_sem=send_sem.at[k],
            recv_sem=recv_sem.at[k],
            device_id=(target,),
            device_id_type=MESH,
        ).start()

    for h in range(8):
        local(qw_hbm.at[:, pl.ds(h * 256, 256)], wcat.at[h, :, pl.ds(0, 256)], 0)
        kv_hbm = kw_hbm if h < 4 else vw_hbm
        local(kv_hbm.at[:, pl.ds((h % 4) * 128, 128)], wcat.at[h, :, pl.ds(256, 128)], 0)
    for h in range(8):
        local(ow_hbm.at[:, pl.ds(h * 256, 256)], owcat.at[h], 1)
    c_kc = local(kc_hbm, kc, 2)
    c_vc = local(vc_hbm, vc, 3)
    c_sg = local(sg_hbm, sg, 4)
    c_su = local(su_hbm, su, 5)
    c_sd = local(sd_hbm, sd, 6)
    c_gate = local(gate_hbm.at[0], gate, 7)
    c_up = local(up_hbm.at[0], up, 8)
    c_down = local(down_hbm.at[0], down, 9)

    barrier = pltpu.get_barrier_semaphore()

    def greet(k, _):
        pl.semaphore_signal(
            barrier, inc=1, device_id=((me + k) % (2 * CHIPS),), device_id_type=MESH
        )
        return 0

    lax.fori_loop(1, 2 * CHIPS, greet, 0)

    wide = hidden_ref[...].astype(F32)
    for s in range(16):
        hid[2 * s : 2 * s + 2, :] = wide[:, 128 * s : 128 * s + 128]
    hidden = hid[...]

    def doubled(gain_ref):
        gdup[pl.ds(0, 16, stride=2), :] = gain_ref[...]
        gdup[pl.ds(1, 16, stride=2), :] = gain_ref[...]
        return gdup[...]

    asend[...] = fold_rms(hidden, doubled(again_ref)).astype(BF16).reshape(4, 8, 128)
    pltpu.make_async_copy(wcat, wcat, local_sem.at[0]).wait()
    pl.semaphore_wait(barrier, 2 * CHIPS - 1)

    def owner_of(k):
        dz, dx, dc = k // 8, (k // 2) % 4, k % 2
        zt, xt, ct = (z + dz) % SIDE, (x + dx) % SIDE, (c + dc) % 2
        return zt, xt * 2 + ct, ((zt * SIDE + y) * SIDE + xt) * 2 + ct

    def holder_of(k):
        dy, dx, dc = k // 8, (k // 2) % 4, k % 2
        yt, xt, ct = (y + dy) % SIDE, (x + dx) % SIDE, (c + dc) % 2
        return xt * 2 + ct, ((z * SIDE + yt) * SIDE + xt) * 2 + ct

    def chip_of(k):
        dz, dy, dx = k // 16, (k // 4) % 4, k % 4
        return (((z + dz) % SIDE) * SIDE + (y + dy) % SIDE) * SIDE + (x + dx) % SIDE

    def send_acts(k, _):
        zt, _, target = owner_of(k)
        remote(asend.at[zt], acts.at[o_me], 0, target)
        return 0

    def send_w(k, _):
        ht, target = holder_of(k)
        remote(wcat.at[ht], wrecv.at[w_me], 1, target)
        return 0

    lax.fori_loop(1, PLANE, send_acts, 0)
    lax.fori_loop(1, PLANE, send_w, 0)
    acts[o_me] = asend[z]
    wrecv[w_me] = wcat[xc]

    lane = lax.broadcasted_iota(jnp.int32, (256, 128), 1)
    tri = (
        lax.broadcasted_iota(jnp.int32, (256, 256), 1)
        <= lax.broadcasted_iota(jnp.int32, (256, 256), 0)
    ).astype(BF16)
    for i in range(2):
        expert = me if i == 0 else partner
        match = routing_ref[...] == expert
        here = jnp.max(jnp.where(match, 1.0, 0.0), axis=1, keepdims=True)
        weight = jnp.sum(jnp.where(match, rweight_ref[...], 0.0), axis=1, keepdims=True)
        spread = jnp.broadcast_to(here, (256, 128))
        place = jnp.dot(tri, spread.astype(BF16), preferred_element_type=F32) - 1.0
        table = jnp.where((place == lane.astype(F32)) & (spread > 0.0), 1.0, 0.0)
        ptmp[...] = table
        for ct in range(4):
            pt[i, ct * 64 : ct * 64 + 64, :] = ptmp[pl.ds(ct, 64, stride=4), :]
        ptmp[...] = jnp.broadcast_to(weight, (256, 128))
        for ct in range(4):
            wtok[i, ct * 64 : ct * 64 + 64, :] = ptmp[pl.ds(ct, 64, stride=4), :]
    ptt[...] = jnp.transpose(pt[0])[0:SLOTS].astype(BF16)

    half_sign = jnp.where(lax.broadcasted_iota(jnp.int32, (1, 128), 1) < 64, -1.0, 1.0)
    turns = []
    for t in range(2):
        angle = len_ref[t].astype(F32) * inv_ref[...]
        turns.append((jnp.cos(angle), jnp.sin(angle) * half_sign))

    def columns_of(arrived):
        xf[...] = arrived[...].astype(F32).reshape(256, 128)
        rows = [
            jnp.concatenate(
                [xf[pl.ds(2 * s + t, 32, stride=8), :] for t in range(2)], axis=0
            )
            for s in range(4)
        ]
        return jnp.concatenate(rows, axis=1).astype(BF16)

    bytes_of(acts, PLANE - 1, recv_sem.at[0])
    bytes_of(wrecv, PLANE - 1, recv_sem.at[1])
    part = jnp.dot(
        columns_of(acts), wrecv[...].reshape(512, 384), preferred_element_type=F32
    )
    for b in range(3):
        for t in range(2):
            p2[pl.ds(2 * b + t, 32, stride=8), :] = part[
                32 * t : 32 * t + 32, 128 * b : 128 * b + 128
            ]
    for t in range(2):
        p2[pl.ds(6 + t, 32, stride=8), :] = jnp.zeros((32, 128), F32)

    def send_part(k, _):
        zt, ht, target = owner_of(k)
        ot = pl.multiple_of((zt * 8 + ht) * 8, 8)
        remote(p2.at[pl.ds(ot, 8), :], qkv_in.at[o_me], 2, target)
        return 0

    lax.fori_loop(1, PLANE, send_part, 0)
    qkv_in[o_me] = p2[pl.ds(pl.multiple_of(o_me * 8, 8), 8), :]

    pltpu.make_async_copy(owcat, owcat, local_sem.at[1]).wait()

    def send_ow(k, _):
        ht, target = holder_of(k)
        remote(owcat.at[ht], owrecv.at[w_me], 3, target)
        return 0

    lax.fori_loop(1, PLANE, send_ow, 0)
    owrecv[w_me] = owcat[xc]
    c_kc.wait()
    c_vc.wait()

    bytes_of(qkv_in, PLANE - 1, recv_sem.at[2])
    total = qkv_in[0:8]
    for k in range(1, 4):
        total = total + qkv_in[8 * k : 8 * k + 8]
    qs[...] = total.reshape(64, 128)

    scale = 128.0**-0.5
    row16 = lax.broadcasted_iota(jnp.int32, (16, 128), 0)
    row8 = lax.broadcasted_iota(jnp.int32, (8, 1), 0)
    lam = jnp.zeros((8, 1), F32)
    for h in range(8):
        lam = jnp.where(row8 == h, lam_ref[h], lam)
    keys, values = [], []
    for t in range(2):
        cos, sin = turns[t]

        def turn(v):
            return v * cos + pltpu.roll(v, 64, 1) * sin

        kv = qs[pl.ds(4 + t, 8, stride=8), :]
        q16 = jnp.concatenate(
            [turn(qs[pl.ds(t, 8, stride=8), :]), turn(qs[pl.ds(2 + t, 8, stride=8), :])],
            axis=0,
        )
        q16 = q16.astype(BF16).astype(F32)
        kn = turn(kv).astype(BF16).astype(F32)
        vn = kv.astype(BF16).astype(F32)
        keys.append(jnp.concatenate([kn[i : i + 1] for i in range(4)], axis=1))
        vflat = jnp.concatenate([vn[i : i + 1] for i in range(4, 8)], axis=1)
        values.append(vflat)
        own_keys = jnp.concatenate(
            [jnp.broadcast_to(kn[i : i + 1], (4, 128)) for i in (0, 2, 1, 3)], axis=0
        )
        self_score = jnp.sum(q16 * own_keys, axis=1, keepdims=True) * scale
        blocks = []
        for k in range(2):
            for j in range(2):
                lo = j * 8 + k * 4
                blocks.append(jnp.where((row16 >= lo) & (row16 < lo + 4), q16, 0.0))
        wide_q = jnp.concatenate(blocks, axis=1).astype(BF16)
        scores = (
            lax.dot_general(
                wide_q, kc[t], (((1,), (1,)), ((), ())), preferred_element_type=F32
            )
            * scale
        )
        live = lax.broadcasted_iota(jnp.int32, (16, 1024), 1) < len_ref[t]
        peak = jnp.maximum(
            jnp.max(jnp.where(live, scores, -jnp.inf), axis=1, keepdims=True), self_score
        )
        weights = jnp.where(live, jnp.exp(scores - peak), 0.0)
        self_w = jnp.exp(self_score - peak)
        totals = jnp.sum(weights, axis=1, keepdims=True) + self_w
        comb = weights[0:8] / totals[0:8] - lam * weights[8:16] / totals[8:16]
        self_comb = self_w[0:8] / totals[0:8] - lam * self_w[8:16] / totals[8:16]
        out = jnp.dot(comb.astype(BF16), vc[t], preferred_element_type=F32)
        out = out + self_comb.astype(BF16).astype(F32) * vflat
        head = jnp.where(row8 < 4, out[:, 0:256], out[:, 256:512])
        mean = jnp.sum(head * head, axis=1, keepdims=True) * (1.0 / 256)
        head = head * lax.rsqrt(mean + eps_head) * hgain_ref[...]
        for half in range(2):
            af[pl.ds(2 * half + t, 8, stride=4), :] = head[:, 128 * half : 128 * half + 128]
    kout_ref[...] = jnp.concatenate(keys, axis=0).astype(BF16)
    vout_ref[...] = jnp.concatenate(values, axis=0).astype(BF16)
    asend2[...] = af[...].astype(BF16).reshape(4, 8, 128)

    def send_acts2(k, _):
        zt, _, target = owner_of(k)
        remote(asend2.at[zt], acts2.at[o_me], 4, target)
        return 0

    lax.fori_loop(1, PLANE, send_acts2, 0)
    acts2[o_me] = asend2[z]
    mgain = doubled(mgain_ref)
    bytes_of(owrecv, PLANE - 1, recv_sem.at[3])
    bytes_of(acts2, PLANE - 1, recv_sem.at[4])
    part = jnp.dot(
        columns_of(acts2), owrecv[...].reshape(512, 256), preferred_element_type=F32
    )
    for b in range(2):
        for t in range(2):
            p5[pl.ds(2 * b + t, 32, stride=8), :] = part[
                32 * t : 32 * t + 32, 128 * b : 128 * b + 128
            ]
    for r in range(4, 8):
        p5[pl.ds(r, 32, stride=8), :] = jnp.zeros((32, 128), F32)

    def send_part2(k, _):
        zt, ht, target = owner_of(k)
        ot = pl.multiple_of((zt * 8 + ht) * 8, 8)
        remote(p5.at[pl.ds(ot, 8), :], oin.at[o_me], 5, target)
        return 0

    lax.fori_loop(1, PLANE, send_part2, 0)
    oin[o_me] = p5[pl.ds(pl.multiple_of(o_me * 8, 8), 8), :]
    bytes_of(oin, PLANE - 1, recv_sem.at[5])
    total = oin[0:8]
    for k in range(1, 4):
        total = total + oin[8 * k : 8 * k + 8]
    for h in range(8):
        proj[4 * h : 4 * h + 4, :] = total[h, 0:4]
    mixed = (hidden + proj[...].astype(BF16).astype(F32)).astype(BF16).astype(F32)
    moe = fold_rms(mixed, mgain).astype(BF16)
    ms[...] = moe

    def send_moe(k, _):
        remote(ms, mrecv.at[c, p], 6, chip_of(k) * 2 + c)
        return 0

    lax.fori_loop(1, CHIPS, send_moe, 0)
    mrecv[c, p] = moe

    moe32 = moe.astype(F32)
    lhs = jnp.concatenate([moe32[2 * s : 2 * s + 2] for s in range(16)], axis=1).astype(BF16)
    c_sg.wait()
    c_su.wait()
    c_sd.wait()
    g = jnp.dot(lhs, sg[...], preferred_element_type=F32)
    u = jnp.dot(lhs, su[...], preferred_element_type=F32)
    shared = jnp.dot(
        (jax.nn.silu(g) * u).astype(BF16), sd[...], preferred_element_type=F32
    )
    for s in range(16):
        shf[2 * s : 2 * s + 2, :] = shared[:, 128 * s : 128 * s + 128]
    c_gate.wait()
    c_up.wait()
    c_down.wait()

    bytes_of(mrecv.at[0], CHIPS - 1, recv_sem.at[6])
    remote(mrecv.at[c], mrecv.at[c], 7, partner)

    def widen_own(i, _):
        big[pl.ds(pl.multiple_of(c * 2048 + i * 128, 128), 128), :] = (
            mrecv[c, pl.ds(i * 4, 4)].astype(F32).reshape(128, 128)
        )
        return 0

    lax.fori_loop(0, 16, widen_own, 0)
    bytes_of(mrecv.at[0], CHIPS, recv_sem.at[7])

    def widen_other(i, _):
        big[pl.ds(pl.multiple_of((1 - c) * 2048 + i * 128, 128), 128), :] = (
            mrecv[1 - c, pl.ds(i * 4, 4)].astype(F32).reshape(128, 128)
        )
        return 0

    lax.fori_loop(0, 16, widen_other, 0)
    for s in range(16):
        rows = jnp.concatenate(
            [
                big[pl.ds((ct // 2) * 2048 + 2 * s + ct % 2, 64, stride=32), :]
                for ct in range(4)
            ],
            axis=0,
        ).astype(BF16)
        pk[:, 128 * s : 128 * s + 128] = jnp.dot(
            ptt[...], rows, preferred_element_type=F32
        ).astype(BF16)
    g = jnp.dot(pk[...], gate[...], preferred_element_type=F32)
    u = jnp.dot(pk[...], up[...], preferred_element_type=F32)
    hidden_e = (jax.nn.silu(g) * u).astype(BF16)
    for i in range(2):
        rs[i] = jnp.dot(
            hidden_e, down[:, 1024 * i : 1024 * i + 1024], preferred_element_type=F32
        ).astype(BF16)

    remote(rs.at[1 - c], rpar, 8, partner)
    own = jnp.dot(pt[0, :, 0:SLOTS].astype(BF16), rs[c], preferred_element_type=F32)
    for ct in range(4):
        for s in range(8):
            big[pl.ds(4 * s + ct, 64, stride=32), :] = (
                own[64 * ct : 64 * ct + 64, 128 * s : 128 * s + 128]
                * wtok[0, 64 * ct : 64 * ct + 64, :]
            )
    bytes_of(rpar, SLOTS, recv_sem.at[8])
    other = jnp.dot(pt[1, :, 0:SLOTS].astype(BF16), rpar[...], preferred_element_type=F32)
    for ct in range(4):
        for s in range(8):
            big[pl.ds(4 * s + ct, 64, stride=32), :] = (
                big[pl.ds(4 * s + ct, 64, stride=32), :]
                + other[64 * ct : 64 * ct + 64, 128 * s : 128 * s + 128]
                * wtok[1, 64 * ct : 64 * ct + 64, :]
            )

    def narrow(i, _):
        esend[pl.ds(i * 4, 4)] = (
            big[pl.ds(pl.multiple_of(i * 128, 128), 128), :].astype(BF16).reshape(4, 32, 128)
        )
        return 0

    lax.fori_loop(0, 16, narrow, 0)

    def send_back(k, _):
        chip = chip_of(k)
        remote(esend.at[chip], erecv.at[p], 9, chip * 2 + c)
        return 0

    lax.fori_loop(1, CHIPS, send_back, 0)
    erecv[p] = esend[p]
    bytes_of(erecv, CHIPS - 1, recv_sem.at[9])

    def add_up(i, acc):
        return acc + jnp.sum(erecv[pl.ds(i * 4, 4)].astype(F32), axis=0)

    total = lax.fori_loop(0, 16, add_up, jnp.zeros((32, 128), F32))
    mine = pl.multiple_of(c * 32, 32)
    es[pl.ds(mine, 32), :] = total
    remote(es.at[pl.ds(mine, 32), :], es.at[pl.ds(mine, 32), :], 10, partner)
    bytes_of(es, 32, recv_sem.at[10])
    for half in range(2):
        for t in range(2):
            rfold[pl.ds(half * 16 + t, 8, stride=2), :] = es[
                pl.ds(half * 32 + c * 2 + t, 8, stride=4), :
            ]
    layer = mixed + rfold[...] + shf[...]
    layer_ref[...] = jnp.concatenate(
        [layer[2 * s : 2 * s + 2] for s in range(16)], axis=1
    ).astype(BF16)

    bytes_of(acts, PLANE - 1, send_sem.at[0])
    bytes_of(wrecv, PLANE - 1, send_sem.at[1])
    bytes_of(qkv_in, PLANE - 1, send_sem.at[2])
    bytes_of(owrecv, PLANE - 1, send_sem.at[3])
    bytes_of(acts2, PLANE - 1, send_sem.at[4])
    bytes_of(oin, PLANE - 1, send_sem.at[5])
    bytes_of(mrecv.at[0], CHIPS - 1, send_sem.at[6])
    bytes_of(mrecv.at[0], CHIPS, send_sem.at[7])
    bytes_of(rpar, SLOTS, send_sem.at[8])
    bytes_of(erecv, CHIPS - 1, send_sem.at[9])
    bytes_of(es, 32, send_sem.at[10])


def on_device(
    hidden_in, lengths, key_cache, value_cache, query_w, key_w, value_w, out_w, lam_heads, head_gain,
    attn_gain, moe_gain, routing, route_weight, gate_w, up_w, down_w, shared_gate, shared_up, shared_down,
):
    inv = (theta_base ** (-np.arange(64, dtype=np.float32) / 64)).astype(np.float32)
    inv = jnp.asarray(np.tile(inv, 2)[None])
    vmem = pl.BlockSpec(memory_space=pltpu.VMEM)
    smem = pl.BlockSpec(memory_space=pltpu.SMEM)
    hbm = pl.BlockSpec(memory_space=pl.ANY)
    V = pltpu.VMEM
    scratch = [
        V((2, 1024, 512), BF16), V((2, 1024, 512), BF16),
        V((D, 512), BF16), V((D, 512), BF16), V((512, D), BF16),
        V((D, 512), BF16), V((D, 512), BF16), V((512, D), BF16),
        V((8, 16, 384), BF16), V((8, 16, 256), BF16), V((32, 16, 384), BF16), V((32, 16, 256), BF16),
        V((32, 128), F32), V((32, 128), F32), V((4, 8, 128), BF16), V((32, 8, 128), BF16),
        V((256, 128), F32), V((256, 128), F32), V((32, 8, 128), F32), V((64, 128), F32),
        V((32, 128), F32), V((4, 8, 128), BF16), V((32, 8, 128), BF16), V((256, 128), F32),
        V((32, 8, 128), F32), V((32, 128), F32),
        V((32, 128), BF16), V((2, 64, 32, 128), BF16), V((4096, 128), F32), V((SLOTS, D), BF16),
        V((2, SLOTS, 1024), BF16), V((SLOTS, 1024), BF16), V((64, 32, 128), BF16), V((64, 32, 128), BF16),
        V((64, 128), F32), V((32, 128), F32), V((32, 128), F32),
        V((2, 256, 128), F32), V((SLOTS, 256), BF16), V((2, 256, 128), F32), V((256, 128), F32),
        pltpu.SemaphoreType.DMA((10,)), pltpu.SemaphoreType.DMA((11,)), pltpu.SemaphoreType.DMA((11,)),
    ]
    return pl.pallas_call(
        kernel,
        out_shape=(
            jax.ShapeDtypeStruct((2, D), BF16),
            jax.ShapeDtypeStruct((2, 512), BF16),
            jax.ShapeDtypeStruct((2, 512), BF16),
        ),
        in_specs=[smem, smem] + [vmem] * 7 + [hbm] * 12,
        out_specs=(vmem, vmem, vmem),
        scratch_shapes=scratch,
        compiler_params=pltpu.CompilerParams(
            collective_id=0, has_side_effects=True, vmem_limit_bytes=56 * 1024 * 1024
        ),
    )(
        lengths, lam_heads, hidden_in, inv,
        attn_gain.reshape(16, 128), moe_gain.reshape(16, 128), head_gain.reshape(1, 256),
        routing, route_weight,
        key_cache, value_cache, query_w, key_w, value_w, out_w, gate_w, up_w, down_w,
        shared_gate, shared_up, shared_down,
    )


def solution(mesh):
    row, cube, whole = P("ep", None), P("ep", None, None), P()
    return jax.shard_map(
        on_device,
        mesh=mesh,
        in_specs=(
            row, P("ep"), cube, cube, row, row, row, row, whole, whole,
            whole, whole, whole, whole, cube, cube, cube, whole, whole, whole,
        ),
        out_specs=(row, row, row),
        check_vma=False,
    )
```

time: 222 us -> 75.4 us (0.34)
  waiting for transfers between devices: 108 us -> 0 us
  Pallas kernels: 0 us -> 67.6 us
  starting transfers between devices: 31.5 us -> 0 us
  blocking collectives: 18.6 us -> 0 us
  matrix products: 17.3 us -> 0 us
  local copies, waits for them, and re-layouts: 20.6 us -> 6.8 us
  between operations: 14.3 us -> 0.64 us
  other arithmetic: 11.2 us -> 0 us
    pallas_call x0 -> x1, Pallas kernels: none -> 67.6 us  [on_device(): pl.pallas_call(kernel, out_shape=(jax.ShapeDtypeStruct((2, D), BF16), jax...]
    all_to_all x5 -> x0, waiting for transfers between devices: 63 us -> none  [the longest x1 18.7 us: on_device(): lax.all_to_all(outgoing, EP, split_axis=0, concat_axis=0, tiled=True)]
    all_gather x1 -> x0, waiting for transfers between devices: 44.1 us -> none  [on_device(): all_rows = lax.all_gather(hidden_in, EP, axis=0, tiled=True)]
    all_to_all x5 -> x0, starting transfers between devices: 31.5 us -> none  [the longest x1 11.5 us: on_device(): lax.all_to_all(joined_rows, EP, split_axis=1, concat_axis=0, tiled=True)]
    all_to_all x2 -> x0, blocking collectives: 18.6 us -> none  [the longest x1 13.7 us: on_device(): lax.all_to_all(attn_out, EP, split_axis=1, concat_axis=0, tiled=True)]
    dot_general x11 -> x0, matrix products: 17.3 us -> none  [the longest x1 3.56 us: on_device(): jnp.dot(shared_hidden, shared_down, preferred_element_type=jnp.float32)]
    reduce_sum x8 -> x0, other arithmetic: 7.08 us -> none  [the longest x1 3.08 us: sent_and_summed(): return arrived.astype(jnp.float32).sum(axis=0)]
    reshape x5 -> x0, local copies, waits for them, and re-layouts: 6.75 us -> none  [the longest x1 3.98 us: attend(): cache_keys = cache_keys.reshape(num_seqs, cache_len, kv_heads, 2, head_dim)]
  transfers between devices with their start and end apart: 6 -> 0, of which waited for: 6 -> 0; matrix products, arithmetic and copies ran while one was open for 5% -> 0% of each run, Pallas kernels for 0% -> 0%
where the time goes in v1:
time: 75.4 us; the launch traced here: 75 us
  Pallas kernels  67.6 us (90%)
  local copies, waits for them, and re-layouts  6.8 us (9%)
    pallas_call x1, Pallas kernels, on_device(): pl.pallas_call(kernel, out_shape=(jax.ShapeDtypeStruct((2, D), BF16), jax...  67.6 us
    unnamed x5, local copies, waits for them, and re-layouts  6.8 us

profile of v1, /device:TPU:1, one launch (start us, length us, event | category | flops | bytes accessed | tf_op | source)
XLA Modules:
  0.0 75.0 jit_solution(6477904467525262803)
XLA Ops:
  0.6 1.5 %copy.24.routing_ref = s32[256,6]{1,0:T(8,128)} copy(s32[256,6]{0,1:T(8,128)} %param.33) | data formatting | bytes 12288 | tf_op args[12]
  2.1 1.5 %copy.25.rweight_ref = f32[256,6]{1,0:T(8,128)} copy(f32[256,6]{0,1:T(8,128)} %param.34) | data formatting | bytes 12288 | tf_op args[13]
  3.6 67.6 %shard_map.220 = (bf16[2,2048]{1,0:T(2,128)(2,1)}, bf16[2,512]{1,0:T(2,128)(2,1)}, bf16[2,512]{1,0:T(2,128)(2,1)}) custom-call(s32[2]{0:T(128)} %len_ref.1, f32[8]{0:T(128)} %lam_ref.1, bf16[2,2048]{1,0:T(2,128)(2,1)} %hidden_ref.1, f32[1,128]{1,0:T(1,128)} %constant.2.clone.inv_ref, f32[16,128]{1,0:T(8,128)} %bitcast.3, f32[16,128]{1,0:T(8,128)} %bitcast.4, ...), custom_call_target="tpu_custom_call" | custom-call | tf_op jit(solution)/shard_map/pallas_call | solution.py:477
  71.2 1.3 %copy.29 = bf16[2,2048]{1,0:T(2,128)(2,1)} copy(bf16[2,2048]{1,0:T(2,128)(2,1)} %get-tuple-element.6) | data formatting | bytes 16384
  72.5 1.3 %copy.30 = bf16[2,512]{1,0:T(2,128)(2,1)} copy(bf16[2,512]{1,0:T(2,128)(2,1)} %get-tuple-element.7) | data formatting | bytes 4096
  73.8 1.3 %copy.31 = bf16[2,512]{1,0:T(2,128)(2,1)} copy(bf16[2,512]{1,0:T(2,128)(2,1)} %get-tuple-element.8) | data formatting | bytes 4096

commit v2 on v1

--- a/solution.py
+++ b/solution.py
@@ -14,6 +14,8 @@
 SIDE = 4
 CHIPS = SIDE**3
 PLANE = SIDE * SIDE * 2
+ISSUE = (2, 1, 3, 0)
+ARRIVE = (1, 3, 0, 2)
 SLOTS = 32
 D = 2048
 eps_norm = 1e-06
@@ -50,7 +52,7 @@
     af, asend2, acts2, p5, oin, proj,
     ms, mrecv, big, pk, rs, rpar, esend, erecv, es, shf, rfold,
     pt, ptt, wtok, ptmp,
-    local_sem, send_sem, recv_sem,
+    local_sem, send_sem, recv_sem, ready_sem,
 ):
     me = lax.axis_index("ep")
     c = me % 2
@@ -78,10 +80,37 @@
             device_id_type=MESH,
         ).start()
 
+    def line_of(k):
+        return ((z * SIDE + y) * SIDE + (x + k // 2) % SIDE) * 2 + (c + k % 2) % 2
+
+    barrier = pltpu.get_barrier_semaphore()
+
+    def greet(sem, target):
+        pl.semaphore_signal(sem, inc=1, device_id=(target,), device_id_type=MESH)
+
+    for k in range(1, 8):
+        greet(barrier, line_of(k))
+    for k in range(1, SIDE):
+        greet(barrier, ((z * SIDE + (y + k) % SIDE) * SIDE + x) * 2 + c)
+        greet(barrier, (((z + k) % SIDE * SIDE + y) * SIDE + x) * 2 + c)
+
     for h in range(8):
         local(qw_hbm.at[:, pl.ds(h * 256, 256)], wcat.at[h, :, pl.ds(0, 256)], 0)
         kv_hbm = kw_hbm if h < 4 else vw_hbm
         local(kv_hbm.at[:, pl.ds((h % 4) * 128, 128)], wcat.at[h, :, pl.ds(256, 128)], 0)
+
+    wide = hidden_ref[...].astype(F32)
+    for s in range(16):
+        hid[2 * s : 2 * s + 2, :] = wide[:, 128 * s : 128 * s + 128]
+    hidden = hid[...]
+
+    def doubled(gain_ref):
+        gdup[pl.ds(0, 16, stride=2), :] = gain_ref[...]
+        gdup[pl.ds(1, 16, stride=2), :] = gain_ref[...]
+        return gdup[...]
+
+    asend[...] = fold_rms(hidden, doubled(again_ref)).astype(BF16).reshape(4, 8, 128)
+    pltpu.make_async_copy(wcat, wcat, local_sem.at[0]).wait()
     for h in range(8):
         local(ow_hbm.at[:, pl.ds(h * 256, 256)], owcat.at[h], 1)
     c_kc = local(kc_hbm, kc, 2)
@@ -93,29 +122,10 @@
     c_up = local(up_hbm.at[0], up, 8)
     c_down = local(down_hbm.at[0], down, 9)
 
-    barrier = pltpu.get_barrier_semaphore()
-
-    def greet(k, _):
-        pl.semaphore_signal(
-            barrier, inc=1, device_id=((me + k) % (2 * CHIPS),), device_id_type=MESH
-        )
-        return 0
-
-    lax.fori_loop(1, 2 * CHIPS, greet, 0)
-
-    wide = hidden_ref[...].astype(F32)
-    for s in range(16):
-        hid[2 * s : 2 * s + 2, :] = wide[:, 128 * s : 128 * s + 128]
-    hidden = hid[...]
-
-    def doubled(gain_ref):
-        gdup[pl.ds(0, 16, stride=2), :] = gain_ref[...]
-        gdup[pl.ds(1, 16, stride=2), :] = gain_ref[...]
-        return gdup[...]
-
-    asend[...] = fold_rms(hidden, doubled(again_ref)).astype(BF16).reshape(4, 8, 128)
-    pltpu.make_async_copy(wcat, wcat, local_sem.at[0]).wait()
-    pl.semaphore_wait(barrier, 2 * CHIPS - 1)
+    pl.semaphore_wait(barrier, 13)
+    for k in range(1, 8):
+        greet(ready_sem, line_of(k))
+    pl.semaphore_wait(ready_sem, 7)
 
     def owner_of(k):
         dz, dx, dc = k // 8, (k // 2) % 4, k % 2
@@ -126,10 +136,6 @@
         dy, dx, dc = k // 8, (k // 2) % 4, k % 2
         yt, xt, ct = (y + dy) % SIDE, (x + dx) % SIDE, (c + dc) % 2
         return xt * 2 + ct, ((z * SIDE + yt) * SIDE + xt) * 2 + ct
-
-    def chip_of(k):
-        dz, dy, dx = k // 16, (k // 4) % 4, k % 4
-        return (((z + dz) % SIDE) * SIDE + (y + dy) % SIDE) * SIDE + (x + dx) % SIDE
 
     def send_acts(k, _):
         zt, _, target = owner_of(k)
@@ -154,15 +160,15 @@
     for i in range(2):
         expert = me if i == 0 else partner
         match = routing_ref[...] == expert
-        here = jnp.max(jnp.where(match, 1.0, 0.0), axis=1, keepdims=True)
-        weight = jnp.sum(jnp.where(match, rweight_ref[...], 0.0), axis=1, keepdims=True)
-        spread = jnp.broadcast_to(here, (256, 128))
+        here = jnp.max(jnp.where(match, 1.0, 0.0), axis=0, keepdims=True)
+        weight = jnp.sum(jnp.where(match, rweight_ref[...], 0.0), axis=0, keepdims=True)
+        spread = jnp.transpose(jnp.broadcast_to(here, (128, 256)))
         place = jnp.dot(tri, spread.astype(BF16), preferred_element_type=F32) - 1.0
         table = jnp.where((place == lane.astype(F32)) & (spread > 0.0), 1.0, 0.0)
         ptmp[...] = table
         for ct in range(4):
             pt[i, ct * 64 : ct * 64 + 64, :] = ptmp[pl.ds(ct, 64, stride=4), :]
-        ptmp[...] = jnp.broadcast_to(weight, (256, 128))
+        ptmp[...] = jnp.transpose(jnp.broadcast_to(weight, (128, 256)))
         for ct in range(4):
             wtok[i, ct * 64 : ct * 64 + 64, :] = ptmp[pl.ds(ct, 64, stride=4), :]
     ptt[...] = jnp.transpose(pt[0])[0:SLOTS].astype(BF16)
@@ -322,11 +328,20 @@
     moe = fold_rms(mixed, mgain).astype(BF16)
     ms[...] = moe
 
-    def send_moe(k, _):
-        remote(ms, mrecv.at[c, p], 6, chip_of(k) * 2 + c)
-        return 0
-
-    lax.fori_loop(1, CHIPS, send_moe, 0)
+    def chip_at(dz, k):
+        zt, yt, xt = (z + dz) % SIDE, (y + k // SIDE) % SIDE, (x + k % SIDE) % SIDE
+        return (zt * SIDE + yt) * SIDE + xt
+
+    def group(dz):
+        return pl.multiple_of((z - dz + SIDE) % SIDE * 16, 16), 16 if dz else 15
+
+    for dz in ISSUE:
+
+        def send_moe(k, _, dz=dz):
+            remote(ms, mrecv.at[c, p], 12 + dz, chip_at(dz, k) * 2 + c)
+            return 0
+
+        lax.fori_loop(0 if dz else 1, 16, send_moe, 0)
     mrecv[c, p] = moe
 
     moe32 = moe.astype(F32)
@@ -345,25 +360,23 @@
     c_up.wait()
     c_down.wait()
 
-    bytes_of(mrecv.at[0], CHIPS - 1, recv_sem.at[6])
-    remote(mrecv.at[c], mrecv.at[c], 7, partner)
-
-    def widen_own(i, _):
-        big[pl.ds(pl.multiple_of(c * 2048 + i * 128, 128), 128), :] = (
-            mrecv[c, pl.ds(i * 4, 4)].astype(F32).reshape(128, 128)
-        )
-        return 0
-
-    lax.fori_loop(0, 16, widen_own, 0)
-    bytes_of(mrecv.at[0], CHIPS, recv_sem.at[7])
-
-    def widen_other(i, _):
-        big[pl.ds(pl.multiple_of((1 - c) * 2048 + i * 128, 128), 128), :] = (
-            mrecv[1 - c, pl.ds(i * 4, 4)].astype(F32).reshape(128, 128)
-        )
-        return 0
-
-    lax.fori_loop(0, 16, widen_other, 0)
+    def widen(core, first):
+        for i in range(4):
+            start = pl.multiple_of(core * 2048 + (first + 4 * i) * 32, 128)
+            big[pl.ds(start, 128), :] = (
+                mrecv[core, pl.ds(first + 4 * i, 4)].astype(F32).reshape(128, 128)
+            )
+
+    for dz in ARRIVE:
+        first, count = group(dz)
+        bytes_of(mrecv.at[0], count, recv_sem.at[12 + dz])
+        block = mrecv.at[c, pl.ds(first, 16)]
+        remote(block, block, 16 + dz, partner)
+        widen(c, first)
+    for dz in ARRIVE:
+        first, _ = group(dz)
+        bytes_of(mrecv.at[0], 16, recv_sem.at[16 + dz])
+        widen(1 - c, first)
     for s in range(16):
         rows = jnp.concatenate(
             [
@@ -401,27 +414,27 @@
                 * wtok[1, 64 * ct : 64 * ct + 64, :]
             )
 
-    def narrow(i, _):
-        esend[pl.ds(i * 4, 4)] = (
-            big[pl.ds(pl.multiple_of(i * 128, 128), 128), :].astype(BF16).reshape(4, 32, 128)
-        )
-        return 0
-
-    lax.fori_loop(0, 16, narrow, 0)
-
-    def send_back(k, _):
-        chip = chip_of(k)
-        remote(esend.at[chip], erecv.at[p], 9, chip * 2 + c)
-        return 0
-
-    lax.fori_loop(1, CHIPS, send_back, 0)
+    for dz in ISSUE:
+        start = (z + dz) % SIDE * 16
+        for i in range(4):
+            rows = pl.multiple_of((start + 4 * i) * 32, 128)
+            esend[pl.ds(start + 4 * i, 4)] = (
+                big[pl.ds(rows, 128), :].astype(BF16).reshape(4, 32, 128)
+            )
+
+        def send_back(k, _, dz=dz):
+            chip = chip_at(dz, k)
+            remote(esend.at[chip], erecv.at[p], 20 + dz, chip * 2 + c)
+            return 0
+
+        lax.fori_loop(0 if dz else 1, 16, send_back, 0)
     erecv[p] = esend[p]
-    bytes_of(erecv, CHIPS - 1, recv_sem.at[9])
-
-    def add_up(i, acc):
-        return acc + jnp.sum(erecv[pl.ds(i * 4, 4)].astype(F32), axis=0)
-
-    total = lax.fori_loop(0, 16, add_up, jnp.zeros((32, 128), F32))
+    total = jnp.zeros((32, 128), F32)
+    for dz in ARRIVE:
+        first, count = group(dz)
+        bytes_of(erecv, count, recv_sem.at[20 + dz])
+        for i in range(4):
+            total = total + jnp.sum(erecv[pl.ds(first + 4 * i, 4)].astype(F32), axis=0)
     mine = pl.multiple_of(c * 32, 32)
     es[pl.ds(mine, 32), :] = total
     remote(es.at[pl.ds(mine, 32), :], es.at[pl.ds(mine, 32), :], 10, partner)
@@ -442,11 +455,18 @@
     bytes_of(owrecv, PLANE - 1, send_sem.at[3])
     bytes_of(acts2, PLANE - 1, send_sem.at[4])
     bytes_of(oin, PLANE - 1, send_sem.at[5])
-    bytes_of(mrecv.at[0], CHIPS - 1, send_sem.at[6])
-    bytes_of(mrecv.at[0], CHIPS, send_sem.at[7])
     bytes_of(rpar, SLOTS, send_sem.at[8])
-    bytes_of(erecv, CHIPS - 1, send_sem.at[9])
     bytes_of(es, 32, send_sem.at[10])
+    for dz in range(SIDE):
+        count = 16 if dz else 15
+        bytes_of(mrecv.at[0], count, send_sem.at[12 + dz])
+        bytes_of(mrecv.at[0], 16, send_sem.at[16 + dz])
+        bytes_of(erecv, count, send_sem.at[20 + dz])
+
+
+def hand_over(*refs):
+    for i in range(3):
+        refs[3 + i][...] = refs[i][...]
 
 
 def on_device(
@@ -472,15 +492,17 @@
         V((2, SLOTS, 1024), BF16), V((SLOTS, 1024), BF16), V((64, 32, 128), BF16), V((64, 32, 128), BF16),
         V((64, 128), F32), V((32, 128), F32), V((32, 128), F32),
         V((2, 256, 128), F32), V((SLOTS, 256), BF16), V((2, 256, 128), F32), V((256, 128), F32),
-        pltpu.SemaphoreType.DMA((10,)), pltpu.SemaphoreType.DMA((11,)), pltpu.SemaphoreType.DMA((11,)),
+        pltpu.SemaphoreType.DMA((10,)), pltpu.SemaphoreType.DMA((24,)), pltpu.SemaphoreType.DMA((24,)),
+        pltpu.SemaphoreType.REGULAR,
     ]
-    return pl.pallas_call(
+    shapes = (
+        jax.ShapeDtypeStruct((2, D), BF16),
+        jax.ShapeDtypeStruct((2, 512), BF16),
+        jax.ShapeDtypeStruct((2, 512), BF16),
+    )
+    results = pl.pallas_call(
         kernel,
-        out_shape=(
-            jax.ShapeDtypeStruct((2, D), BF16),
-            jax.ShapeDtypeStruct((2, 512), BF16),
-            jax.ShapeDtypeStruct((2, 512), BF16),
-        ),
+        out_shape=shapes,
         in_specs=[smem, smem] + [vmem] * 7 + [hbm] * 12,
         out_specs=(vmem, vmem, vmem),
         scratch_shapes=scratch,
@@ -490,10 +512,13 @@
     )(
         lengths, lam_heads, hidden_in, inv,
         attn_gain.reshape(16, 128), moe_gain.reshape(16, 128), head_gain.reshape(1, 256),
-        routing, route_weight,
+        routing.T, route_weight.T,
         key_cache, value_cache, query_w, key_w, value_w, out_w, gate_w, up_w, down_w,
         shared_gate, shared_up, shared_down,
     )
+    return pl.pallas_call(
+        hand_over, out_shape=shapes, in_specs=[vmem] * 3, out_specs=(vmem,) * 3
+    )(*results)
 
 
 def solution(mesh):

time: 75.4 us -> 66 us (0.88)
  local copies, waits for them, and re-layouts: 6.8 us -> 0 us
  Pallas kernels: 67.6 us -> 65.1 us
    unnamed x5 -> x0, local copies, waits for them, and re-layouts: 6.8 us -> none
    pallas_call x1 -> x2, Pallas kernels: 67.6 us -> 65.1 us  [the longest x1 63.8 us: on_device(): pl.pallas_call(kernel, out_shape=shapes, in_specs=[smem, smem] + [vmem] *...]
where the time goes in v2:
time: 66 us; the launch traced here: 65.8 us
  Pallas kernels  65.1 us (99%)
    pallas_call x1, Pallas kernels, on_device(): pl.pallas_call(kernel, out_shape=shapes, in_specs=[smem, smem] + [vmem] *...  63.8 us

profile of v2, /device:TPU:1, one launch (start us, length us, event | category | flops | bytes accessed | tf_op | source)
XLA Modules:
  0.0 65.8 jit_solution(328838639496139564)
XLA Ops:
  0.6 63.8 %shard_map.220 = (bf16[2,2048]{1,0:T(2,128)(2,1)}, bf16[2,512]{1,0:T(2,128)(2,1)}, bf16[2,512]{1,0:T(2,128)(2,1)}) custom-call(s32[2]{0:T(128)} %len_ref.1, f32[8]{0:T(128)} %lam_ref.1, bf16[2,2048]{1,0:T(2,128)(2,1)} %hidden_ref.1, f32[1,128]{1,0:T(1,128)} %constant.2.clone.inv_ref, f32[16,128]{1,0:T(8,128)} %bitcast.5, f32[16,128]{1,0:T(8,128)} %bitcast.6, ...), custom_call_target="tpu_custom_call" | custom-call | tf_op jit(solution)/shard_map/pallas_call | solution.py:503
  64.5 1.3 %shard_map.221 = (bf16[2,2048]{1,0:T(2,128)(2,1)}, bf16[2,512]{1,0:T(2,128)(2,1)}, bf16[2,512]{1,0:T(2,128)(2,1)}) custom-call(bf16[2,2048]{1,0:T(2,128)(2,1)} %get-tuple-element.6.refs_0_, bf16[2,512]{1,0:T(2,128)(2,1)} %get-tuple-element.7.refs_1_, bf16[2,512]{1,0:T(2,128)(2,1)} %get-tuple-element.8.refs_2_), custom_call_target="tpu_custom_call" | custom-call | tf_op jit(solution)/shard_map/pallas_call | solution.py:519

commit v3 on v2

--- a/solution.py
+++ b/solution.py
@@ -50,8 +50,8 @@
     wcat, owcat, wrecv, owrecv,
     hid, gdup, asend, acts, xf, p2, qkv_in, qs,
     af, asend2, acts2, p5, oin, proj,
-    ms, mrecv, big, pk, rs, rpar, esend, erecv, es, shf, rfold,
-    pt, ptt, wtok, ptmp,
+    ms, mrecv, big, pk, pgive, ptake, rs, rpar, esend, erecv, shf,
+    pt, ptt, ptmp,
     local_sem, send_sem, recv_sem, ready_sem,
 ):
     me = lax.axis_index("ep")
@@ -152,26 +152,31 @@
     acts[o_me] = asend[z]
     wrecv[w_me] = wcat[xc]
 
-    lane = lax.broadcasted_iota(jnp.int32, (256, 128), 1)
-    tri = (
-        lax.broadcasted_iota(jnp.int32, (256, 256), 1)
-        <= lax.broadcasted_iota(jnp.int32, (256, 256), 0)
+    upto = (
+        lax.broadcasted_iota(jnp.int32, (256, 256), 0)
+        <= lax.broadcasted_iota(jnp.int32, (256, 256), 1)
     ).astype(BF16)
-    for i in range(2):
-        expert = me if i == 0 else partner
+    slot = lax.broadcasted_iota(jnp.int32, (SLOTS, 256), 0).astype(F32)
+    tables = []
+    for expert in (me, partner):
         match = routing_ref[...] == expert
         here = jnp.max(jnp.where(match, 1.0, 0.0), axis=0, keepdims=True)
-        weight = jnp.sum(jnp.where(match, rweight_ref[...], 0.0), axis=0, keepdims=True)
-        spread = jnp.transpose(jnp.broadcast_to(here, (128, 256)))
-        place = jnp.dot(tri, spread.astype(BF16), preferred_element_type=F32) - 1.0
-        table = jnp.where((place == lane.astype(F32)) & (spread > 0.0), 1.0, 0.0)
-        ptmp[...] = table
+        rows = jnp.broadcast_to(here, (8, 256)).astype(BF16)
+        place = jnp.dot(rows, upto, preferred_element_type=F32)[0:1] - 1.0
+        tables.append(jnp.where((place == slot) & (here > 0.0), 1.0, 0.0))
+        if expert is me:
+            weight = jnp.sum(jnp.where(match, rweight_ref[...], 0.0), axis=0, keepdims=True)
+            slot_w = jnp.sum(tables[0] * weight, axis=1, keepdims=True)
+    tables.append(jnp.zeros((128 - 2 * SLOTS, 256), F32))
+    ptmp[...] = jnp.transpose(jnp.concatenate(tables, axis=0))
+    for zq in range(SIDE):
         for ct in range(4):
-            pt[i, ct * 64 : ct * 64 + 64, :] = ptmp[pl.ds(ct, 64, stride=4), :]
-        ptmp[...] = jnp.transpose(jnp.broadcast_to(weight, (128, 256)))
-        for ct in range(4):
-            wtok[i, ct * 64 : ct * 64 + 64, :] = ptmp[pl.ds(ct, 64, stride=4), :]
-    ptt[...] = jnp.transpose(pt[0])[0:SLOTS].astype(BF16)
+            at = zq * 64 + ct * 16
+            pt[at : at + 16, :] = ptmp[pl.ds(zq * 64 + ct, 16, stride=4), :]
+    seen = jnp.concatenate(
+        [ptmp[pl.ds(c * 2 + t, 64, stride=4), :] for t in range(2)], axis=0
+    )
+    ptt[...] = jnp.transpose(seen)[0 : 2 * SLOTS].astype(BF16)
 
     half_sign = jnp.where(lax.broadcasted_iota(jnp.int32, (1, 128), 1) < 64, -1.0, 1.0)
     turns = []
@@ -338,11 +343,11 @@
     for dz in ISSUE:
 
         def send_moe(k, _, dz=dz):
-            remote(ms, mrecv.at[c, p], 12 + dz, chip_at(dz, k) * 2 + c)
+            remote(ms, mrecv.at[p], 12 + dz, chip_at(dz, k) * 2 + c)
             return 0
 
         lax.fori_loop(0 if dz else 1, 16, send_moe, 0)
-    mrecv[c, p] = moe
+    mrecv[p] = moe
 
     moe32 = moe.astype(F32)
     lhs = jnp.concatenate([moe32[2 * s : 2 * s + 2] for s in range(16)], axis=1).astype(BF16)
@@ -360,91 +365,75 @@
     c_up.wait()
     c_down.wait()
 
-    def widen(core, first):
-        for i in range(4):
-            start = pl.multiple_of(core * 2048 + (first + 4 * i) * 32, 128)
-            big[pl.ds(start, 128), :] = (
-                mrecv[core, pl.ds(first + 4 * i, 4)].astype(F32).reshape(128, 128)
-            )
-
     for dz in ARRIVE:
         first, count = group(dz)
-        bytes_of(mrecv.at[0], count, recv_sem.at[12 + dz])
-        block = mrecv.at[c, pl.ds(first, 16)]
-        remote(block, block, 16 + dz, partner)
-        widen(c, first)
-    for dz in ARRIVE:
-        first, _ = group(dz)
-        bytes_of(mrecv.at[0], 16, recv_sem.at[16 + dz])
-        widen(1 - c, first)
-    for s in range(16):
+        bytes_of(mrecv, count, recv_sem.at[12 + dz])
+        for i in range(4):
+            start = pl.multiple_of((first + 4 * i) * 32, 128)
+            big[pl.ds(start, 128), :] = (
+                mrecv[pl.ds(first + 4 * i, 4)].astype(F32).reshape(128, 128)
+            )
+    for s in range(8):
         rows = jnp.concatenate(
             [
-                big[pl.ds((ct // 2) * 2048 + 2 * s + ct % 2, 64, stride=32), :]
-                for ct in range(4)
+                jnp.concatenate(
+                    [big[pl.ds(4 * s + 2 * i + t, 64, stride=32), :] for t in range(2)], axis=0
+                )
+                for i in range(2)
             ],
-            axis=0,
+            axis=1,
         ).astype(BF16)
-        pk[:, 128 * s : 128 * s + 128] = jnp.dot(
-            ptt[...], rows, preferred_element_type=F32
-        ).astype(BF16)
+        picked = jnp.dot(ptt[...], rows, preferred_element_type=F32).astype(BF16)
+        pk[:, 256 * s : 256 * s + 256] = picked[0:SLOTS]
+        pgive[:, 256 * s : 256 * s + 256] = picked[SLOTS : 2 * SLOTS]
+    remote(pgive, ptake, 7, partner)
+    bytes_of(ptake, SLOTS, recv_sem.at[7])
+    pk[...] = (pk[...].astype(F32) + ptake[...].astype(F32)).astype(BF16)
     g = jnp.dot(pk[...], gate[...], preferred_element_type=F32)
     u = jnp.dot(pk[...], up[...], preferred_element_type=F32)
     hidden_e = (jax.nn.silu(g) * u).astype(BF16)
     for i in range(2):
-        rs[i] = jnp.dot(
+        made = jnp.dot(
             hidden_e, down[:, 1024 * i : 1024 * i + 1024], preferred_element_type=F32
         ).astype(BF16)
+        rs[i] = (made.astype(F32) * slot_w).astype(BF16)
 
     remote(rs.at[1 - c], rpar, 8, partner)
-    own = jnp.dot(pt[0, :, 0:SLOTS].astype(BF16), rs[c], preferred_element_type=F32)
-    for ct in range(4):
-        for s in range(8):
-            big[pl.ds(4 * s + ct, 64, stride=32), :] = (
-                own[64 * ct : 64 * ct + 64, 128 * s : 128 * s + 128]
-                * wtok[0, 64 * ct : 64 * ct + 64, :]
+    bytes_of(rpar, SLOTS, recv_sem.at[8])
+    pair = jnp.concatenate([rs[c], rpar[...]], axis=0)
+    for dz in ISSUE:
+        zt = (z + dz) % SIDE
+        rows = pt[pl.ds(pl.multiple_of(zt * 64, 64), 64), 0 : 2 * SLOTS].astype(BF16)
+        both = jnp.dot(rows, pair, preferred_element_type=F32)
+        for ct in range(4):
+            for s in range(8):
+                big[pl.ds(dz * 512 + (ct // 2) * 16 + 2 * s + ct % 2, 16, stride=32), :] = both[
+                    16 * ct : 16 * ct + 16, 128 * s : 128 * s + 128
+                ]
+        for i in range(4):
+            at = dz * 512 + i * 128
+            esend[pl.ds((zt * 16 + 4 * i) * 2, 8)] = (
+                big[at : at + 128, :].astype(BF16).reshape(8, 16, 128)
             )
-    bytes_of(rpar, SLOTS, recv_sem.at[8])
-    other = jnp.dot(pt[1, :, 0:SLOTS].astype(BF16), rpar[...], preferred_element_type=F32)
-    for ct in range(4):
-        for s in range(8):
-            big[pl.ds(4 * s + ct, 64, stride=32), :] = (
-                big[pl.ds(4 * s + ct, 64, stride=32), :]
-                + other[64 * ct : 64 * ct + 64, 128 * s : 128 * s + 128]
-                * wtok[1, 64 * ct : 64 * ct + 64, :]
-            )
-
-    for dz in ISSUE:
-        start = (z + dz) % SIDE * 16
-        for i in range(4):
-            rows = pl.multiple_of((start + 4 * i) * 32, 128)
-            esend[pl.ds(start + 4 * i, 4)] = (
-                big[pl.ds(rows, 128), :].astype(BF16).reshape(4, 32, 128)
-            )
 
         def send_back(k, _, dz=dz):
-            chip = chip_at(dz, k)
-            remote(esend.at[chip], erecv.at[p], 20 + dz, chip * 2 + c)
+            chip, core = chip_at(dz, k // 2), (c + k % 2) % 2
+            device = chip * 2 + core
+            remote(esend.at[device], erecv.at[c * CHIPS + p], 20 + dz, device)
             return 0
 
-        lax.fori_loop(0 if dz else 1, 16, send_back, 0)
-    erecv[p] = esend[p]
-    total = jnp.zeros((32, 128), F32)
+        lax.fori_loop(0 if dz else 1, 32, send_back, 0)
+    erecv[c * CHIPS + p] = esend[me]
+    halves = [jnp.zeros((16, 128), F32)] * 2
     for dz in ARRIVE:
         first, count = group(dz)
-        bytes_of(erecv, count, recv_sem.at[20 + dz])
-        for i in range(4):
-            total = total + jnp.sum(erecv[pl.ds(first + 4 * i, 4)].astype(F32), axis=0)
-    mine = pl.multiple_of(c * 32, 32)
-    es[pl.ds(mine, 32), :] = total
-    remote(es.at[pl.ds(mine, 32), :], es.at[pl.ds(mine, 32), :], 10, partner)
-    bytes_of(es, 32, recv_sem.at[10])
-    for half in range(2):
-        for t in range(2):
-            rfold[pl.ds(half * 16 + t, 8, stride=2), :] = es[
-                pl.ds(half * 32 + c * 2 + t, 8, stride=4), :
-            ]
-    layer = mixed + rfold[...] + shf[...]
+        bytes_of(erecv, 16 + count, recv_sem.at[20 + dz])
+        for half in range(2):
+            for i in range(2):
+                rows = erecv[pl.ds(half * CHIPS + first + 8 * i, 8)].astype(F32)
+                halves[half] = halves[half] + jnp.sum(rows, axis=0)
+    routed = jnp.concatenate(halves, axis=0)
+    layer = mixed + routed + shf[...]
     layer_ref[...] = jnp.concatenate(
         [layer[2 * s : 2 * s + 2] for s in range(16)], axis=1
     ).astype(BF16)
@@ -455,13 +444,12 @@
     bytes_of(owrecv, PLANE - 1, send_sem.at[3])
     bytes_of(acts2, PLANE - 1, send_sem.at[4])
     bytes_of(oin, PLANE - 1, send_sem.at[5])
+    bytes_of(ptake, SLOTS, send_sem.at[7])
     bytes_of(rpar, SLOTS, send_sem.at[8])
-    bytes_of(es, 32, send_sem.at[10])
     for dz in range(SIDE):
         count = 16 if dz else 15
-        bytes_of(mrecv.at[0], count, send_sem.at[12 + dz])
-        bytes_of(mrecv.at[0], 16, send_sem.at[16 + dz])
-        bytes_of(erecv, count, send_sem.at[20 + dz])
+        bytes_of(mrecv, count, send_sem.at[12 + dz])
+        bytes_of(erecv, 16 + count, send_sem.at[20 + dz])
 
 
 def hand_over(*refs):
@@ -488,10 +476,11 @@
         V((256, 128), F32), V((256, 128), F32), V((32, 8, 128), F32), V((64, 128), F32),
         V((32, 128), F32), V((4, 8, 128), BF16), V((32, 8, 128), BF16), V((256, 128), F32),
         V((32, 8, 128), F32), V((32, 128), F32),
-        V((32, 128), BF16), V((2, 64, 32, 128), BF16), V((4096, 128), F32), V((SLOTS, D), BF16),
-        V((2, SLOTS, 1024), BF16), V((SLOTS, 1024), BF16), V((64, 32, 128), BF16), V((64, 32, 128), BF16),
-        V((64, 128), F32), V((32, 128), F32), V((32, 128), F32),
-        V((2, 256, 128), F32), V((SLOTS, 256), BF16), V((2, 256, 128), F32), V((256, 128), F32),
+        V((32, 128), BF16), V((64, 32, 128), BF16), V((2048, 128), F32), V((SLOTS, D), BF16), V((SLOTS, D), BF16),
+        V((SLOTS, D), BF16),
+        V((2, SLOTS, 1024), BF16), V((SLOTS, 1024), BF16), V((128, 16, 128), BF16), V((128, 16, 128), BF16),
+        V((32, 128), F32),
+        V((256, 128), F32), V((2 * SLOTS, 128), BF16), V((256, 128), F32),
         pltpu.SemaphoreType.DMA((10,)), pltpu.SemaphoreType.DMA((24,)), pltpu.SemaphoreType.DMA((24,)),
         pltpu.SemaphoreType.REGULAR,
     ]

time: 66 us -> 63.3 us (0.959)
  Pallas kernels: 65.1 us -> 62.4 us
    pallas_call x1, Pallas kernels: 63.8 us -> 61.1 us  [on_device(): pl.pallas_call(kernel, out_shape=shapes, in_specs=[smem, smem] + [vmem] *...]
where the time goes in v3:
time: 63.3 us; the launch traced here: 63 us
  Pallas kernels  62.4 us (99%)
  between operations  0.65 us (1%)
    pallas_call x1, Pallas kernels, on_device(): pl.pallas_call(kernel, out_shape=shapes, in_specs=[smem, smem] + [vmem] *...  61.1 us
    pallas_call x1, Pallas kernels, on_device(): pl.pallas_call(hand_over, out_shape=shapes, in_specs=[vmem] * 3, out_spec...  1.31 us

profile of v3, /device:TPU:1, one launch (start us, length us, event | category | flops | bytes accessed | tf_op | source)
XLA Modules:
  0.0 63.0 jit_solution(3007429481572383022)
XLA Ops:
  0.6 61.1 %shard_map.220 = (bf16[2,2048]{1,0:T(2,128)(2,1)}, bf16[2,512]{1,0:T(2,128)(2,1)}, bf16[2,512]{1,0:T(2,128)(2,1)}) custom-call(s32[2]{0:T(128)} %len_ref.1, f32[8]{0:T(128)} %lam_ref.1, bf16[2,2048]{1,0:T(2,128)(2,1)} %hidden_ref.1, f32[1,128]{1,0:T(1,128)} %constant.2.clone.inv_ref, f32[16,128]{1,0:T(8,128)} %bitcast.5, f32[16,128]{1,0:T(8,128)} %bitcast.6, ...), custom_call_target="tpu_custom_call" | custom-call | tf_op jit(solution)/shard_map/pallas_call | solution.py:492
  61.7 1.3 %shard_map.221 = (bf16[2,2048]{1,0:T(2,128)(2,1)}, bf16[2,512]{1,0:T(2,128)(2,1)}, bf16[2,512]{1,0:T(2,128)(2,1)}) custom-call(bf16[2,2048]{1,0:T(2,128)(2,1)} %get-tuple-element.6.refs_0_, bf16[2,512]{1,0:T(2,128)(2,1)} %get-tuple-element.7.refs_1_, bf16[2,512]{1,0:T(2,128)(2,1)} %get-tuple-element.8.refs_2_), custom_call_target="tpu_custom_call" | custom-call | tf_op jit(solution)/shard_map/pallas_call | solution.py:508

commit v4 on v3

--- a/solution.py
+++ b/solution.py
@@ -309,26 +309,21 @@
     )
     for b in range(2):
         for t in range(2):
-            p5[pl.ds(2 * b + t, 32, stride=8), :] = part[
-                32 * t : 32 * t + 32, 128 * b : 128 * b + 128
-            ]
-    for r in range(4, 8):
-        p5[pl.ds(r, 32, stride=8), :] = jnp.zeros((32, 128), F32)
+            p5[:, 2 * b + t, :] = part[32 * t : 32 * t + 32, 128 * b : 128 * b + 128]
 
     def send_part2(k, _):
         zt, ht, target = owner_of(k)
-        ot = pl.multiple_of((zt * 8 + ht) * 8, 8)
-        remote(p5.at[pl.ds(ot, 8), :], oin.at[o_me], 5, target)
+        remote(p5.at[zt * 8 + ht], oin.at[o_me], 5, target)
         return 0
 
     lax.fori_loop(1, PLANE, send_part2, 0)
-    oin[o_me] = p5[pl.ds(pl.multiple_of(o_me * 8, 8), 8), :]
+    oin[o_me] = p5[o_me]
     bytes_of(oin, PLANE - 1, recv_sem.at[5])
     total = oin[0:8]
     for k in range(1, 4):
         total = total + oin[8 * k : 8 * k + 8]
     for h in range(8):
-        proj[4 * h : 4 * h + 4, :] = total[h, 0:4]
+        proj[4 * h : 4 * h + 4, :] = total[h]
     mixed = (hidden + proj[...].astype(BF16).astype(F32)).astype(BF16).astype(F32)
     moe = fold_rms(mixed, mgain).astype(BF16)
     ms[...] = moe
@@ -474,8 +469,8 @@
         V((8, 16, 384), BF16), V((8, 16, 256), BF16), V((32, 16, 384), BF16), V((32, 16, 256), BF16),
         V((32, 128), F32), V((32, 128), F32), V((4, 8, 128), BF16), V((32, 8, 128), BF16),
         V((256, 128), F32), V((256, 128), F32), V((32, 8, 128), F32), V((64, 128), F32),
-        V((32, 128), F32), V((4, 8, 128), BF16), V((32, 8, 128), BF16), V((256, 128), F32),
-        V((32, 8, 128), F32), V((32, 128), F32),
+        V((32, 128), F32), V((4, 8, 128), BF16), V((32, 8, 128), BF16), V((32, 4, 128), F32),
+        V((32, 4, 128), F32), V((32, 128), F32),
         V((32, 128), BF16), V((64, 32, 128), BF16), V((2048, 128), F32), V((SLOTS, D), BF16), V((SLOTS, D), BF16),
         V((SLOTS, D), BF16),
         V((2, SLOTS, 1024), BF16), V((SLOTS, 1024), BF16), V((128, 16, 128), BF16), V((128, 16, 128), BF16),

time: 63.3 us -> 63.1 us (level)
  no operation moved by 1% of the time
where the time goes in v4:
time: 63.1 us; the launch traced here: 62.8 us
  Pallas kernels  62.2 us (99%)
  between operations  0.65 us (1%)
    pallas_call x1, Pallas kernels, on_device(): pl.pallas_call(kernel, out_shape=shapes, in_specs=[smem, smem] + [vmem] *...  60.9 us
    pallas_call x1, Pallas kernels, on_device(): pl.pallas_call(hand_over, out_shape=shapes, in_specs=[vmem] * 3, out_spec...  1.31 us

profile of v4, /device:TPU:1, one launch (start us, length us, event | category | flops | bytes accessed | tf_op | source)
XLA Modules:
  0.0 62.8 jit_solution(12921696291652680256)
XLA Ops:
  0.6 60.9 %shard_map.220 = (bf16[2,2048]{1,0:T(2,128)(2,1)}, bf16[2,512]{1,0:T(2,128)(2,1)}, bf16[2,512]{1,0:T(2,128)(2,1)}) custom-call(s32[2]{0:T(128)} %len_ref.1, f32[8]{0:T(128)} %lam_ref.1, bf16[2,2048]{1,0:T(2,128)(2,1)} %hidden_ref.1, f32[1,128]{1,0:T(1,128)} %constant.2.clone.inv_ref, f32[16,128]{1,0:T(8,128)} %bitcast.5, f32[16,128]{1,0:T(8,128)} %bitcast.6, ...), custom_call_target="tpu_custom_call" | custom-call | tf_op jit(solution)/shard_map/pallas_call | solution.py:487
  61.5 1.3 %shard_map.221 = (bf16[2,2048]{1,0:T(2,128)(2,1)}, bf16[2,512]{1,0:T(2,128)(2,1)}, bf16[2,512]{1,0:T(2,128)(2,1)}) custom-call(bf16[2,2048]{1,0:T(2,128)(2,1)} %get-tuple-element.6.refs_0_, bf16[2,512]{1,0:T(2,128)(2,1)} %get-tuple-element.7.refs_1_, bf16[2,512]{1,0:T(2,128)(2,1)} %get-tuple-element.8.refs_2_), custom_call_target="tpu_custom_call" | custom-call | tf_op jit(solution)/shard_map/pallas_call | solution.py:503
